TPU v7x, 32 devices: a whole 2x2x4 slice. The times are simulated.
32 devices in a mesh: sp: 16 (over z, y, x), tp: 2 (over core).
Axes of the slice: x: 2, y: 2, z: 4, core: 2. Of those that a mesh axis runs over, the one named last changes fastest.
Arguments:
- resid: bfloat16 [2048, 2048], P('sp', 'tp'), may hold values from -6 to 6
- qa_nope: bfloat16 [2048, 1024], P('sp', 'tp'), may hold values from -6 to 6
- qb_nope: bfloat16 [2048, 1024], P('sp', 'tp'), may hold values from -6 to 6
- qa_rope: bfloat16 [2048, 512], P('sp', 'tp'), may hold values from -360 to 360
- qb_rope: bfloat16 [2048, 256], P('sp', 'tp'), may hold values from -360 to 360
- latent: bfloat16 [2048, 256], P('sp'), may hold values from -6 to 6
- key_rope: bfloat16 [2048, 32], P('sp'), may hold values from -4 to 4
- lat_gain: float32 [256], replicated, may hold values from 0.1 to 1.9
- wa_key: bfloat16 [256, 1024], P(None, 'tp'), may hold values from -0.375 to 0.375
- wa_val: bfloat16 [256, 1024], P(None, 'tp'), may hold values from -0.75 to 0.75
- wb_key: bfloat16 [256, 1024], P(None, 'tp'), may hold values from -0.375 to 0.375
- wb_val: bfloat16 [256, 1024], P(None, 'tp'), may hold values from -0.75 to 0.75
- gain_a: float32 [1024], P('tp'), may hold values from 0.1 to 1.9
- gain_b: float32 [1024], P('tp'), may hold values from 0.1 to 1.9
- wa_out: bfloat16 [1024, 2048], P('tp'), may hold values from -0.125 to 0.125
- wb_out: bfloat16 [1024, 2048], P('tp'), may hold values from -0.125 to 0.125
- norm1_gain: float32 [2048], replicated, may hold values from 0.1 to 1.9
- ffn_gate: bfloat16 [2048, 5632], P('sp', 'tp'), may hold values from -0.125 to 0.125
- ffn_val: bfloat16 [2048, 5632], P('sp', 'tp'), may hold values from -0.125 to 0.125
- conv_gate: float32 [3, 5632], P(None, 'tp'), may hold values from -3 to 3
- conv_val: float32 [3, 5632], P(None, 'tp'), may hold values from -3 to 3
- ffn_down: bfloat16 [5632, 2048], P('tp'), may hold values from -0.078125 to 0.078125
- norm2_gain: float32 [2048], P('tp'), may hold values from 0.1 to 1.9
Outputs:
- layer_out: bfloat16 [2048, 2048], P('sp', 'tp')
All inputs are finite; a program needn't handle non-finite values.
Results may differ from a plain program's by a relative error of at most 0.017.
Values may be sent and summed in bfloat16 or wider, within the bound.
A program may use at most 128 MiB of HBM per device.

v0:
```python
import jax
import jax.numpy as jnp
from jax import lax
from jax.sharding import PartitionSpec as P

D = 2048
HA = 16
DA = 64
HB = 8
DB = 128
DR = 32
KC = 3


THETA = 10000.0
EPS_RMS = 1e-06
EPS_NORM = 1e-05
ALPHA = 2.0**0.25


def passed_along(value, axis, steps):
    count = lax.axis_size(axis)
    leading, last = (max(0, -steps), min(count, count - steps))
    return lax.ppermute(value, axis, [(source, source + steps) for source in range(leading, last)])


def rotary(values, positions):
    half = values.shape[-1] // 2
    freq = THETA ** (-jnp.arange(half, dtype=jnp.float32) * 2.0 / values.shape[-1])
    angle = positions.astype(jnp.float32)[:, None] * freq[None, :]
    if values.ndim == 3:
        angle = angle[:, None, :]
    cosine = jnp.cos(angle)
    sine = jnp.sin(angle)
    first = values[..., :half]
    second = values[..., half:]
    return jnp.concatenate(
        [first * cosine - second * sine, second * cosine + first * sine], axis=-1
    )


def rms_scale(values, gain):
    wide = values.astype(jnp.float32)
    return wide * lax.rsqrt(jnp.mean(wide * wide, axis=-1, keepdims=True) + EPS_RMS) * gain


def finish_norm(values, sums, gain, width):
    center = sums[0] / width
    spread = sums[1] / width - center * center
    return (values - center[:, None]) * lax.rsqrt(spread + EPS_NORM)[:, None] * gain


def start_carry(count, heads, width):
    return (
        jnp.full((heads, count), -1e30, jnp.float32),
        jnp.zeros((heads, count), jnp.float32),
        jnp.zeros((count, heads, width), jnp.float32),
    )


def divide_total(carry):
    mixed = carry[2] / jnp.transpose(carry[1])[:, :, None]
    return mixed.reshape(mixed.shape[0], mixed.shape[1] * mixed.shape[2])


def causal_taps(extended, taps, count):
    total = jnp.zeros((count, extended.shape[1]), jnp.float32)
    for tap in range(KC):
        total = total + taps[tap] * extended[tap : tap + count].astype(jnp.float32)
    return total


def shards(
    resid,
    qa_nope,
    qb_nope,
    qa_rope,
    qb_rope,
    latent,
    key_rope,
    lat_gain,
    wa_key,
    wa_val,
    wb_key,
    wb_val,
    gain_a,
    gain_b,
    wa_out,
    wb_out,
    norm1_gain,
    ffn_gate,
    ffn_val,
    conv_gate,
    conv_val,
    ffn_down,
    norm2_gain,
):
    tok_rows = resid.shape[0]
    positions = lax.axis_index("sp") * tok_rows + jnp.arange(tok_rows)
    heads_a = qa_nope.shape[1] // DA
    heads_b = qb_nope.shape[1] // DB
    lat_n = rms_scale(latent, lat_gain).astype(jnp.bfloat16)
    k_rot = rotary(key_rope.astype(jnp.float32), positions).astype(jnp.bfloat16)
    rot_a = rotary(qa_rope.astype(jnp.float32).reshape(tok_rows, heads_a, DR), positions).astype(
        jnp.bfloat16
    )
    rot_b = rotary(qb_rope.astype(jnp.float32).reshape(tok_rows, heads_b, DR), positions).astype(
        jnp.bfloat16
    )
    query_a = qa_nope.reshape(tok_rows, heads_a, DA)
    query_b = qb_nope.reshape(tok_rows, heads_b, DB)

    def absorb(carry, query, q_rot, keys, k_part, vals):
        width = query.shape[2]
        scale = (width + DR) ** (-0.5)
        count = keys.shape[0]
        scores = jnp.einsum("qhd,khd->hqk", query, keys, preferred_element_type=jnp.float32)
        scores = (
            scores + jnp.einsum("qhr,kr->hqk", q_rot, k_part, preferred_element_type=jnp.float32)
        ) * scale
        key_pos = jnp.arange(count)
        allowed = key_pos[None, :] <= positions[:, None]
        scores = jnp.where(allowed[None], scores, -1e30)
        top_old, total_old, running_old = carry
        top_new = jnp.maximum(top_old, jnp.max(scores, axis=-1))
        weights = jnp.exp(scores - top_new[:, :, None])
        total_new = jnp.sum(weights, axis=-1)
        update = jnp.einsum(
            "hqk,khd->qhd", weights.astype(jnp.bfloat16), vals, preferred_element_type=jnp.float32
        )
        return (top_new, total_new, update)

    def project(source, weight, heads, width):
        result = jnp.dot(source, weight, preferred_element_type=jnp.float32).astype(jnp.bfloat16)
        return result.reshape(source.shape[0], heads, width)

    empty = (start_carry(tok_rows, heads_a, DA), start_carry(tok_rows, heads_b, DB))
    pieces = (
        lax.all_gather(lat_n, "sp", axis=0, tiled=True),
        lax.all_gather(k_rot, "sp", axis=0, tiled=True),
    )
    first_group = absorb(
        empty[0],
        query_a,
        rot_a,
        project(pieces[0], wa_key, heads_a, DA),
        pieces[1],
        project(pieces[0], wa_val, heads_a, DA),
    )
    second_group = absorb(
        empty[1],
        query_b,
        rot_b,
        project(pieces[0], wb_key, heads_b, DB),
        pieces[1],
        project(pieces[0], wb_val, heads_b, DB),
    )
    raw_a = divide_total(first_group)
    raw_b = divide_total(second_group)
    local_energy = jnp.sum(raw_a * raw_a, axis=1) + jnp.sum(raw_b * raw_b, axis=1)
    energy = lax.psum(local_energy, "tp")
    head_factor = lax.rsqrt(energy / (HA * DA + HB * DB) + EPS_RMS)[:, None]
    out_a = (raw_a * head_factor * gain_a).astype(jnp.bfloat16)
    out_b = (raw_b * head_factor * gain_b).astype(jnp.bfloat16)
    partial_value = jnp.dot(out_a, wa_out, preferred_element_type=jnp.float32) + jnp.dot(
        out_b, wb_out, preferred_element_type=jnp.float32
    )
    columns = resid.shape[1]
    mix_cols = lax.psum_scatter(
        partial_value.astype(jnp.bfloat16), "tp", scatter_dimension=1, tiled=True
    ).astype(jnp.float32)
    pre_one = ALPHA * resid.astype(jnp.float32) + mix_cols
    sums_one = lax.psum((jnp.sum(pre_one, axis=1), jnp.sum(pre_one * pre_one, axis=1)), "tp")
    gain_cols = lax.dynamic_slice_in_dim(norm1_gain, lax.axis_index("tp") * columns, columns, 0)
    first_cols = finish_norm(pre_one, sums_one, gain_cols, D).astype(jnp.bfloat16)
    first_full = lax.all_gather(first_cols, "tp", axis=1, tiled=True)
    pieces = (
        lax.all_gather(ffn_gate, "sp", axis=0, tiled=True),
        lax.all_gather(ffn_val, "sp", axis=0, tiled=True),
    )
    count = pieces[0].shape[0]
    gate_sum = jnp.dot(first_full, pieces[0], preferred_element_type=jnp.float32)
    val_sum = jnp.dot(first_full, pieces[1], preferred_element_type=jnp.float32)
    gate_up = gate_sum.astype(jnp.bfloat16)
    val_up = val_sum.astype(jnp.bfloat16)
    rim_gate, rim_val = passed_along(
        (gate_up[tok_rows - (KC - 1) :], val_up[tok_rows - (KC - 1) :]), "sp", 1
    )
    gate_c = causal_taps(jnp.concatenate([rim_gate, gate_up], axis=0), conv_gate, tok_rows)
    val_c = causal_taps(jnp.concatenate([rim_val, val_up], axis=0), conv_val, tok_rows)
    hidden = (jax.nn.silu(gate_c) * val_c).astype(jnp.bfloat16)
    down = jnp.dot(hidden, ffn_down, preferred_element_type=jnp.float32)
    ff_cols = lax.psum_scatter(
        down.astype(jnp.bfloat16), "tp", scatter_dimension=1, tiled=True
    ).astype(jnp.float32)
    pre_two = ALPHA * first_cols.astype(jnp.float32) + ff_cols
    sums_two = lax.psum((jnp.sum(pre_two, axis=1), jnp.sum(pre_two * pre_two, axis=1)), "tp")
    return finish_norm(pre_two, sums_two, norm2_gain, D).astype(jnp.bfloat16)


def solution(mesh):
    return jax.shard_map(
        shards,
        mesh=mesh,
        in_specs=(
            P("sp", "tp"),
            P("sp", "tp"),
            P("sp", "tp"),
            P("sp", "tp"),
            P("sp", "tp"),
            P("sp", None),
            P("sp", None),
            P(),
            P(None, "tp"),
            P(None, "tp"),
            P(None, "tp"),
            P(None, "tp"),
            P("tp"),
            P("tp"),
            P("tp", None),
            P("tp", None),
            P(),
            P("sp", "tp"),
            P("sp", "tp"),
            P(None, "tp"),
            P(None, "tp"),
            P("tp", None),
            P("tp"),
        ),
        out_specs=P("sp", "tp"),
        check_vma=False,
    )
```

profile of v0, /device:TPU:31, one launch (start us, length us, event | category | flops | bytes accessed | tf_op | source)
XLA Modules:
  0.0 420.2 jit_solution(2568383577491744750)
XLA Ops:
  7.6 1.6 fusion.46
  13.0 29.1 %all_gather.16 = bf16[2048,32]{0,1:T(8,128)(2,1)S(1)} all-gather(bf16[128,32]{0,1:T(8,128)(2,1)S(1)} %pad_maximum_fusion.4), channel_id=1, replica_groups=mesh['sp'=16,'tp'=2] {'sp'}, dimensions={0}, use_global_device_ids=true | all-gather | bytes 139264 | tf_op jit(solution)/shard_map/all_gather | solution.py:140
  42.4 19.9 %all-gather.4.cloned.1.call-done = bf16[2048,256]{1,0:T(8,128)(2,1)} async-done(((bf16[128,256]{1,0:T(8,128)(2,1)}), bf16[2048,256]{1,0:T(8,128)(2,1)}) %all-gather.4.cloned.1.call-update) | async-done | bytes 1048592 | tf_op jit(solution)/shard_map/all_gather | solution.py:139
  62.2 2.0 convolution_convert_fusion.2
  67.2 1.4 fusion.65
  68.6 1.8 fusion.64
  74.9 1.6 multiply_reduce_fusion.3
  76.6 5.1 %psum.35 = f32[128]{0:T(128)S(1)} all-reduce(f32[128]{0:T(128)S(1)} %add.103), channel_id=1, replica_groups=mesh['sp'=16,'tp'=2] {'tp'}, use_global_device_ids=true, to_apply=%region_7.8 | all-reduce | flops 128 | bytes 1024 | tf_op jit(solution)/shard_map/psum | solution.py:161
  83.3 1.3 fusion.11
  86.0 8.0 %reduce-scatter.3.cloned.1.call-done = bf16[128,1024]{1,0:T(8,128)(2,1)} async-done(((bf16[128,2048]{1,0:T(8,128)(2,1)}), bf16[128,1024]{1,0:T(8,128)(2,1)}) %reduce-scatter.3.cloned.1.call-update) | async-done | bytes 262160 | tf_op jit(solution)/shard_map/reduce_scatter | solution.py:169
  94.0 1.1 fusion.38
  95.1 2.5 all-reduce.1
  98.7 2.2 all_gather.17
  100.9 134.9 %all-gather.8.cloned.1.call-done = bf16[2048,2816]{1,0:T(8,128)(2,1)} async-done(((bf16[128,2816]{1,0:T(8,128)(2,1)}), bf16[2048,2816]{1,0:T(8,128)(2,1)}) %all-gather.8.cloned.1.call-update) | async-done | bytes 11534352 | tf_op jit(solution)/shard_map/all_gather | solution.py:179
  235.8 5.9 %convolution_convert_fusion = bf16[128,2816]{1,0:T(8,128)(2,1)S(1)} fusion(bf16[128,2048]{1,0:T(8,128)(2,1)S(1)} %all_gather.17, bf16[2048,2816]{1,0:T(8,128)(2,1)} %all-gather.8.cloned.1.call-done), kind=kOutput, calls=%fused_computation.14 | convolution fusion | flops 1476755456 | bytes 12779520 | tf_op jit(solution)/shard_map/dot_general | solution.py:183
  241.8 1.4 collective-permute-start.1
  243.3 134.8 %all-gather.6.cloned.1.call-done = bf16[2048,2816]{1,0:T(8,128)(2,1)} async-done(((bf16[128,2816]{1,0:T(8,128)(2,1)}), bf16[2048,2816]{1,0:T(8,128)(2,1)}) %all-gather.6.cloned.1.call-update) | async-done | bytes 11534352 | tf_op jit(solution)/shard_map/all_gather | solution.py:178
  378.1 5.9 %convolution_convert_fusion.1 = bf16[128,2816]{1,0:T(8,128)(2,1)S(1)} fusion(bf16[128,2048]{1,0:T(8,128)(2,1)S(1)} %all_gather.17, bf16[2048,2816]{1,0:T(8,128)(2,1)} %all-gather.6.cloned.1.call-done), kind=kOutput, calls=%fused_computation.15 | convolution fusion | flops 1476755456 | bytes 12779520 | tf_op jit(solution)/shard_map/dot_general | solution.py:182
  384.0 1.3 collective-permute-start
  385.6 2.9 collective-permute-done
  388.5 7.9 %convolution_convert_fusion.6 = bf16[128,2048]{1,0:T(8,128)(2,1)} fusion(bf16[2816,2048]{1,0:T(8,128)(2,1)} %param.44, bf16[128,2816]{1,0:T(8,128)(2,1)S(1)} %convolution_convert_fusion, bf16[128,2816]{1,0:T(8,128)(2,1)S(1)} %convolution_convert_fusion.1, bf16[2,2816]{1,0:T(2,128)(2,1)S(1)} %collective-permute-done.1, ...), kind=kOutput, calls=%fused_computation.22 | convolution fusion | flops 1488912384 | bytes 13590528 | tf_op jit(solution)/shard_map/dot_general | solution.py:192
  396.4 11.8 %reduce-scatter.5.cloned.1.call-done = bf16[128,1024]{1,0:T(8,128)(2,1)} async-done(((bf16[128,2048]{1,0:T(8,128)(2,1)}), bf16[128,1024]{1,0:T(8,128)(2,1)}) %reduce-scatter.5.cloned.1.call-update) | async-done | bytes 262160 | tf_op jit(solution)/shard_map/reduce_scatter | solution.py:193
  409.4 2.5 all-reduce
  411.9 1.8 multiply_convert_fusion.2
  (77 shorter events, 17.8 us)
Async XLA Ops:
  6.5 75.4 %copy-start = (bf16[512,2048]{1,0:T(8,128)(2,1)S(1)}, bf16[512,2048]{1,0:T(8,128)(2,1)}, u32[]{:S(2)}) copy-start(bf16[512,2048]{1,0:T(8,128)(2,1)} %param.37) | copy-start | bytes 6291460
  6.5 55.7 %all-gather.4.cloned.1.call-start = ((), (), s32[]{:S(2)}) async-start(), calls=%async_computation.2 | async-start | bytes 1114112 | tf_op jit(solution)/shard_map/all_gather | solution.py:139
  9.2 84.7 %reduce-scatter.3.cloned.1.call-start = ((), (), s32[]{:S(2)}) async-start(), calls=%async_computation.3 | async-start | bytes 786432 | tf_op jit(solution)/shard_map/reduce_scatter | solution.py:169
  12.9 51.4 %copy-start.8 = (bf16[128,512]{1,0:T(8,128)(2,1)S(1)}, bf16[128,512]{1,0:T(8,128)(2,1)}, u32[]{:S(2)}) copy-start(bf16[128,512]{1,0:T(8,128)(2,1)} %param.25) | copy-start | bytes 393220
  65.2 1.2 copy-start.2
  65.2 1.3 copy-start.5
  70.4 1.0 copy-start.6
  73.0 1.1 copy-start.7
  74.9 6.8 %copy-start.12 = (f32[512]{0:T(512)S(1)}, f32[512]{0:T(512)}, u32[]{:S(2)}) copy-start(f32[512]{0:T(512)} %param.36) | copy-start | bytes 6148
  74.9 6.8 %copy-start.13 = (f32[512]{0:T(512)S(1)}, f32[512]{0:T(512)}, u32[]{:S(2)}) copy-start(f32[512]{0:T(512)} %param.35) | copy-start | bytes 6148
  81.7 1.6 copy-start.3
  83.2 2.7 copy-start.14
  83.2 10.7 %copy-start.4 = (bf16[128,1024]{1,0:T(8,128)(2,1)S(1)}, bf16[128,1024]{1,0:T(8,128)(2,1)}, u32[]{:S(2)}) copy-start(bf16[128,1024]{1,0:T(8,128)(2,1)} %param.23) | copy-start | bytes 786436
  84.6 151.3 %all-gather.8.cloned.1.call-start = ((), (), s32[]{:S(2)}) async-start(), calls=%async_computation.5 | async-start | bytes 12255232 | tf_op jit(solution)/shard_map/all_gather | solution.py:179
  85.3 292.8 %all-gather.6.cloned.1.call-start = ((), (), s32[]{:S(2)}) async-start(), calls=%async_computation.4 | async-start | bytes 12255232 | tf_op jit(solution)/shard_map/all_gather | solution.py:178
  85.9 322.3 %reduce-scatter.5.cloned.1.call-start = ((), (), s32[]{:S(2)}) async-start(), calls=%async_computation.6 | async-start | bytes 786432 | tf_op jit(solution)/shard_map/reduce_scatter | solution.py:193
  241.8 143.6 %copy-start.9 = (f32[3,2816]{1,0:T(4,128)S(1)}, f32[3,2816]{1,0:T(4,128)}, u32[]{:S(2)}) copy-start(f32[3,2816]{1,0:T(4,128)} %param.43) | copy-start | bytes 101380
  241.8 143.5 %copy-start.10 = (f32[3,2816]{1,0:T(4,128)S(1)}, f32[3,2816]{1,0:T(4,128)}, u32[]{:S(2)}) copy-start(f32[3,2816]{1,0:T(4,128)} %param.42) | copy-start | bytes 101380
  241.8 143.7 %collective-permute-start.1 = (bf16[2,2816]{1,0:T(2,128)(2,1)S(1)}, bf16[2,2816]{1,0:T(2,128)(2,1)S(1)}, u32[]{:S(2)}, u32[]{:S(2)}) collective-permute-start(bf16[2,2816]{1,0:T(2,128)(2,1)S(1)} %slice.81), channel_id=1, source_target_pairs={{0,2},{2,4},{4,6},{6,8},{8,10},{10,12},{12,14},{14,16},{16,18},{18... | collective-permute-start | bytes 33800 | tf_op jit(solution)/shard_map/ppermute | solution.py:24
  384.0 4.4 %collective-permute-start = (bf16[2,2816]{1,0:T(2,128)(2,1)S(1)}, bf16[2,2816]{1,0:T(2,128)(2,1)S(1)}, u32[]{:S(2)}, u32[]{:S(2)}) collective-permute-start(bf16[2,2816]{1,0:T(2,128)(2,1)S(1)} %slice.78), channel_id=1, source_target_pairs={{0,2},{2,4},{4,6},{6,8},{8,10},{10,12},{12,14},{14,16},{16,18},{18... | collective-permute-start | bytes 33800 | tf_op jit(solution)/shard_map/ppermute | solution.py:24
  388.5 23.4 %copy-start.11 = (f32[1024]{0:T(1024)S(1)}, f32[1024]{0:T(1024)}, u32[]{:S(2)}) copy-start(f32[1024]{0:T(1024)} %param.45) | copy-start | bytes 12292
  388.5 25.2 %copy-start.1 = (bf16[512,2048]{1,0:T(8,128)(2,1)S(1)}, bf16[512,2048]{1,0:T(8,128)(2,1)}, u32[]{:S(2)}) copy-start(bf16[512,2048]{1,0:T(8,128)(2,1)} %param.37) | copy-start | bytes 6291460
Sparse Core Ops, SparseCore 0:
  10.1 52.0 all-gather.3
  84.7 9.2 reduce-scatter.2
  96.7 139.0 all-gather.7
  238.4 139.5 all-gather.5
  396.6 11.6 reduce-scatter.4
where the time goes:
time: 422 us; the launch traced here: 420 us
  waiting for transfers between devices  314 us (74%)
  blocking collectives  41.3 us (10%)
  matrix products  33.3 us (8%)
  between operations  13.5 us (3%)
  other arithmetic  10.8 us (3%)
  local copies, waits for them, and re-layouts  4.69 us (1%)
    all_gather x1, waiting for transfers between devices, shards(): lax.all_gather(ffn_val, 'sp', axis=0, tiled=True)  135 us
    all_gather x1, waiting for transfers between devices, shards(): lax.all_gather(ffn_gate, 'sp', axis=0, tiled=True)  135 us
    all_gather x1, blocking collectives, shards(): lax.all_gather(k_rot, 'sp', axis=0, tiled=True)  29.1 us
    all_gather x1, waiting for transfers between devices, shards(): lax.all_gather(lat_n, 'sp', axis=0, tiled=True)  19.9 us
    reduce_scatter x1, waiting for transfers between devices, shards(): lax.psum_scatter(down.astype(jnp.bfloat16), 'tp', scatter_dimension=1, ti...  11.8 us
  transfers between devices with their start and end apart: 7, of which 6 were waited for; matrix products, arithmetic and copies ran while one was open for 4% of the time, Pallas kernels for 0%

commit v1 on v0

--- a/solution.py
+++ b/solution.py
@@ -1,6 +1,10 @@
+import functools
+
 import jax
 import jax.numpy as jnp
 from jax import lax
+from jax.experimental import pallas as pl
+from jax.experimental.pallas import tpu as pltpu
 from jax.sharding import PartitionSpec as P
 
 D = 2048
@@ -68,6 +72,510 @@
     for tap in range(KC):
         total = total + taps[tap] * extended[tap : tap + count].astype(jnp.float32)
     return total
+
+
+BF = jnp.bfloat16
+BF = jnp.bfloat16
+LANES = 128
+MESH = pl.DeviceIdType.MESH
+
+
+def greet(n, tp):
+    me, core = lax.axis_index("sp"), lax.axis_index("tp")
+    barrier = pltpu.get_barrier_semaphore()
+    for step in range(1, n):
+        pl.semaphore_signal(
+            barrier, inc=1, device_id=(lax.rem(me + step, n), core), device_id_type=MESH
+        )
+    pl.semaphore_signal(barrier, inc=1, device_id=(me, 1 - core), device_id_type=MESH)
+    pl.semaphore_wait(barrier, n)
+
+
+def send(src, dst, send_sem, recv_sem, sp, core):
+    return pltpu.make_async_remote_copy(
+        src_ref=src,
+        dst_ref=dst,
+        send_sem=send_sem,
+        recv_sem=recv_sem,
+        device_id=(sp, core),
+        device_id_type=MESH,
+    )
+
+
+def block_order(n, me):
+    depth = n // 4
+    zi = me // 4
+    if depth == 4:
+        order = [zi, zi + 1 - 2 * lax.rem(zi, 2), 3 - zi, lax.rem(zi + 2, 4)]
+        return order, order
+    order = [lax.rem(zi + d, depth) for d in range(depth)]
+    return order, [lax.rem(zi + depth - d, depth) for d in range(depth)]
+
+
+class Gather:
+    def __init__(self, n, own, full, sems):
+        self.me, self.core = lax.axis_index("sp"), lax.axis_index("tp")
+        me = self.me
+        self.depth = n // 4
+        self.own, self.full, self.sems = own, full, sems
+        xi, yi = lax.rem(me, 2), lax.rem(me // 2, 2)
+        self.x_peer, self.y_peer = me + 1 - 2 * xi, me + 2 - 4 * yi
+        self.offs = [lax.rem(me, 4), lax.rem(self.x_peer, 4), lax.rem(self.y_peer, 4)]
+        self.offs.append(3 - self.offs[0])
+        self.order, self.targets = block_order(n, me)
+        half = full.shape[2]
+        cut = (half // 2 + 15) // 16 * 16
+        self.cuts = (pl.ds(0, cut), pl.ds(cut, half - cut))
+        self.started = []
+        self.lines = [
+            send(
+                own.at[self.core],
+                full.at[me, self.core],
+                sems[0].at[d],
+                sems[1].at[d],
+                self.targets[d] * 4 + self.offs[0],
+                self.core,
+            )
+            for d in range(1, self.depth)
+        ]
+
+    def block(self, d, place):
+        return self.order[d] * 4 + self.offs[place]
+
+    def share(self, d, place):
+        block = self.block(d, place)
+        ref = self.full.at[block, self.core]
+        pair = self.sems[10], self.sems[11]
+        return send(ref, ref, pair[0].at[block], pair[1].at[block], self.me, 1 - self.core)
+
+    def across(self, d, x_way):
+        ref = self.full.at[self.block(d, 0), self.core]
+        src = self.own.at[self.core] if d == 0 else ref
+        at = 2 if x_way else 4
+        peer = self.x_peer if x_way else self.y_peer
+        return send(src, ref, self.sems[at].at[d], self.sems[at + 1].at[d], peer, self.core)
+
+    def corner(self, d, x_way):
+        block = self.block(d, 2 if x_way else 1)
+        ref = self.full.at[block, self.core, self.cuts[0 if x_way else 1]]
+        at = 6 if x_way else 8
+        peer = self.x_peer if x_way else self.y_peer
+        return send(ref, ref, self.sems[at].at[d], self.sems[at + 1].at[d], peer, self.core)
+
+    def go(self, copy):
+        copy.start()
+        self.started.append(copy)
+
+    def stage_a(self, d):
+        if d > 0:
+            self.lines[d - 1].wait_recv()
+        self.go(self.across(d, True))
+        self.go(self.across(d, False))
+        if d == 0:
+            for copy in self.lines:
+                copy.start()
+        else:
+            self.go(self.share(d, 0))
+
+    def stage_b(self, d):
+        self.across(d, True).wait_recv()
+        self.go(self.corner(d, False))
+        self.go(self.share(d, 1))
+        self.across(d, False).wait_recv()
+        self.go(self.corner(d, True))
+        self.go(self.share(d, 2))
+
+    def stage_c(self, d):
+        self.corner(d, True).wait_recv()
+        self.corner(d, False).wait_recv()
+        self.go(self.share(d, 3))
+
+    def arrived(self, d):
+        for place in range(4):
+            if d or place:
+                self.share(d, place).wait_recv()
+
+    def run(self, use, before=None):
+        stages = ((self.stage_a, 0), (self.stage_b, 1), (self.stage_c, 2), (use, 3))
+        for tick in range(self.depth + 3):
+            for stage, lag in stages:
+                if 0 <= tick - lag < self.depth:
+                    stage(tick - lag)
+            if tick == 0 and before is not None:
+                before()
+
+    def finish(self):
+        for copy in self.lines + self.started:
+            copy.wait_send()
+
+
+def layer_kernel(
+    n,
+    lat_ref,
+    qa_ref,
+    qb_ref,
+    ra_ref,
+    rb_ref,
+    cos_ref,
+    sin_ref,
+    wak_ref,
+    wav_ref,
+    wbk_ref,
+    wbv_ref,
+    gain_a_ref,
+    gain_b_ref,
+    resid_ref,
+    gain1_ref,
+    taps_ref,
+    gain2_ref,
+    out_a_hbm,
+    out_b_hbm,
+    down_hbm,
+    columns_hbm,
+    out_ref,
+    lats,
+    kk,
+    att_a,
+    att_b,
+    out_a_w,
+    out_b_w,
+    weight_ref,
+    part_ref,
+    part_in,
+    energy_ref,
+    energy_in,
+    resid_in,
+    first_ref,
+    full,
+    ups,
+    hidden_out,
+    hidden_in,
+    down_ref,
+    sums_out,
+    sums_in,
+    pre_ref,
+    load_sem,
+    pair_s,
+    pair_r,
+    w_s,
+    w_r,
+    h_s,
+    h_r,
+    *gather_sems,
+):
+    me, core = lax.axis_index("sp"), lax.axis_index("tp")
+    rows, columns = resid_ref.shape
+    half_rows = rows // 2
+    width = part_ref.shape[1]
+    cols = hidden_in.shape[1]
+
+    def piece(chip):
+        return columns_hbm.at[:, pl.ds(pl.multiple_of(chip * cols, 16), cols), :]
+
+    place = weight_ref.at[:, :, pl.ds(pl.multiple_of(me * rows, rows), rows)]
+    own_w = pltpu.make_async_copy(piece(me), place, load_sem.at[0])
+    loads = [
+        own_w,
+        pltpu.make_async_copy(out_a_hbm, out_a_w, load_sem.at[1]),
+        pltpu.make_async_copy(out_b_hbm, out_b_w, load_sem.at[2]),
+        pltpu.make_async_copy(down_hbm, down_ref, load_sem.at[3]),
+    ]
+    for copy in loads:
+        copy.start()
+    lats[me] = lat_ref[...]
+    greet(n, 2)
+    swap_resid = send(resid_ref, resid_in, pair_s.at[2], pair_r.at[2], me, 1 - core)
+    w_copies = []
+    for step in range(1, n):
+        to = lax.rem(me + step, n)
+        w_copies.append(send(piece(to), place, w_s.at[step], w_r.at[step], to, core))
+
+    def behind_latents():
+        swap_resid.start()
+
+    lat_gather = Gather(n, lat_ref, lats, gather_sems[:12])
+
+    def nothing(d):
+        lat_gather.arrived(d)
+
+    lat_gather.run(nothing, behind_latents)
+    for copy in w_copies:
+        copy.start()
+
+    splits = (lats.shape[1] * lats.shape[2] - rows * DR // LANES) // rows
+    lat_width = splits * LANES
+    groups = LANES // DR
+    group_rows = rows // groups
+    into = lax.broadcasted_iota(jnp.int32, (LANES, LANES), 0)
+    lane = lax.broadcasted_iota(jnp.int32, (LANES, LANES), 1)
+
+    def lay_out(block, carry):
+        flat = lats[block].reshape(-1, LANES)
+        for at in range(splits):
+            kk[block, :, at * LANES : (at + 1) * LANES] = flat[at * rows : (at + 1) * rows]
+        packed = flat[splits * rows :]
+        for group in range(groups):
+            pick = (into == group * DR + lax.rem(lane, DR)).astype(jnp.float32).astype(BF)
+            kk[block, group * group_rows : (group + 1) * group_rows, lat_width:] = jnp.dot(
+                packed, pick, preferred_element_type=jnp.float32
+            ).astype(BF)
+        return carry
+
+    lax.fori_loop(0, n, lay_out, 0)
+
+    total_keys = n * rows
+    q_pos = me * rows + lax.broadcasted_iota(jnp.int32, (rows, total_keys), 0)
+    k_pos = lax.broadcasted_iota(jnp.int32, (rows, total_keys), 1)
+    tile_lane = lax.broadcasted_iota(jnp.int32, (rows, LANES), 1)
+
+    def head(h, q_ref, rot_ref, key_ref, val_ref, size, acc):
+        scale = (size + DR) ** (-0.5)
+        of_head = lax.broadcasted_iota(jnp.int32, q_ref.shape, 1) // size == h
+        query = jnp.where(of_head, q_ref[...].astype(jnp.float32), 0.0).astype(BF)
+        absorbed = lax.dot_general(
+            query, key_ref[...], (((1,), (1,)), ((), ())), preferred_element_type=jnp.float32
+        ).astype(BF)
+        tile = rot_ref[:, pl.ds(pl.multiple_of((h // groups) * LANES, LANES), LANES)]
+        tile = tile.astype(jnp.float32)
+        swapped = jnp.where(
+            lax.rem(tile_lane, DR) < DR // 2,
+            pltpu.roll(tile, LANES - DR // 2, 1),
+            pltpu.roll(tile, DR // 2, 1),
+        )
+        turned = tile * cos_ref[...] + swapped * sin_ref[...]
+        turned = jnp.where(tile_lane // DR == lax.rem(h, groups), turned, 0.0).astype(BF)
+        both = jnp.concatenate([absorbed, turned], axis=1)
+        keys = kk[...].reshape(total_keys, lat_width + LANES)
+        scores = (
+            lax.dot_general(
+                both, keys, (((1,), (1,)), ((), ())), preferred_element_type=jnp.float32
+            )
+            * scale
+        )
+        scores = jnp.where(k_pos <= q_pos, scores, -1e30)
+        weights = jnp.exp(scores - jnp.max(scores, axis=1, keepdims=True))
+        total = jnp.sum(weights, axis=1, keepdims=True)
+        mixed = jnp.dot(
+            weights.astype(BF), keys[:, :lat_width], preferred_element_type=jnp.float32
+        )
+        values = jnp.dot(
+            (mixed / total).astype(BF), val_ref[...], preferred_element_type=jnp.float32
+        )
+        acc[...] = jnp.where(of_head, values, acc[...])
+
+    def heads_a(h, carry):
+        head(h, qa_ref, ra_ref, wak_ref, wav_ref, DA, att_a)
+        return carry
+
+    def heads_b(h, carry):
+        head(h, qb_ref, rb_ref, wbk_ref, wbv_ref, DB, att_b)
+        return carry
+
+    att_a[...] = jnp.zeros_like(att_a)
+    att_b[...] = jnp.zeros_like(att_b)
+    lax.fori_loop(0, qa_ref.shape[1] // DA, heads_a, 0)
+    lax.fori_loop(0, qb_ref.shape[1] // DB, heads_b, 0)
+    raw_a, raw_b = att_a[...], att_b[...]
+    local = jnp.sum(raw_a * raw_a, axis=1, keepdims=True)
+    local = local + jnp.sum(raw_b * raw_b, axis=1, keepdims=True)
+    energy_ref[...] = jnp.broadcast_to(local, energy_ref.shape)
+    give_a = (raw_a * gain_a_ref[...]).astype(BF)
+    give_b = (raw_b * gain_b_ref[...]).astype(BF)
+    loads[1].wait()
+    loads[2].wait()
+    part_ref[...] = (
+        jnp.dot(give_a, out_a_w[...], preferred_element_type=jnp.float32)
+        + jnp.dot(give_b, out_b_w[...], preferred_element_type=jnp.float32)
+    ).astype(BF)
+    pair = [
+        send(part_ref, part_in, pair_s.at[0], pair_r.at[0], me, 1 - core),
+        send(energy_ref, energy_in, pair_s.at[1], pair_r.at[1], me, 1 - core),
+    ]
+    for copy in pair:
+        copy.start()
+    for copy in pair:
+        copy.wait()
+    swap_resid.wait()
+    low = (core == 0).astype(jnp.float32)
+    mine = resid_ref[...].astype(jnp.float32)
+    other = resid_in[...].astype(jnp.float32)
+    resid = jnp.concatenate(
+        [mine * low + other * (1.0 - low), other * low + mine * (1.0 - low)], axis=1
+    )
+    energy = (energy_ref[...] + energy_in[...])[:, :1]
+    factor = lax.rsqrt(energy / (HA * DA + HB * DB) + EPS_RMS)
+    mix = (part_ref[...].astype(jnp.float32) + part_in[...].astype(jnp.float32)) * factor
+    pre = ALPHA * resid + mix
+    shifted = pre - jnp.mean(pre, axis=1, keepdims=True)
+    spread = jnp.mean(shifted * shifted, axis=1, keepdims=True)
+    first = (shifted * lax.rsqrt(spread + EPS_NORM) * gain1_ref[...]).astype(BF)
+    first_ref[...] = first.reshape(2, half_rows, width)
+    full[me] = first.reshape(2, half_rows, width)
+
+    gather = Gather(n, first_ref, full, gather_sems[12:])
+
+    def project_up(d):
+        gather.arrived(d)
+        if d == 0:
+            for copy in w_copies:
+                copy.wait()
+            own_w.wait()
+        base = gather.order[d] * 4
+
+        def one(step, carry):
+            block = base + step
+            up = lax.dot_general(
+                weight_ref[...].reshape(2 * cols, width),
+                full[block].reshape(rows, width),
+                (((1,), (1,)), ((), ())),
+                preferred_element_type=jnp.float32,
+            )
+            ups[block] = up.astype(BF)
+            return carry
+
+        lax.fori_loop(0, 4, one, 0)
+
+    gather.run(project_up)
+
+    lane = lax.broadcasted_iota(jnp.int32, (2 * cols, rows), 1)
+
+    def hidden_copy(block):
+        return send(
+            hidden_out.at[block], hidden_in.at[me], h_s.at[block], h_r.at[me], block, core
+        )
+
+    def convolve(block, before):
+        current = ups[block].astype(jnp.float32)
+        total = taps_ref[:, KC - 1 : KC] * current
+        for back in range(1, KC):
+            moved = jnp.where(
+                lane < back, pltpu.roll(before, back, 1), pltpu.roll(current, back, 1)
+            )
+            total = total + taps_ref[:, KC - 1 - back : KC - back] * moved
+        gate, val = total[:cols], total[cols:]
+        hidden = gate / (1.0 + jnp.exp(-gate)) * val
+        hidden_out[block] = hidden.astype(BF)
+
+        @pl.when(block == me)
+        def _():
+            hidden_in[block] = hidden.astype(BF)
+
+        @pl.when((block > 0) & (block - 1 != me))
+        def _():
+            hidden_copy(block - 1).start()
+
+        return current
+
+    lax.fori_loop(0, n, convolve, jnp.zeros((2 * cols, rows), jnp.float32))
+
+    @pl.when(me != n - 1)
+    def _():
+        hidden_copy(n - 1).start()
+
+    gather.finish()
+    lat_gather.finish()
+
+    for step in range(1, n):
+        source = lax.rem(me + step, n)
+        send(
+            hidden_out.at[source],
+            hidden_in.at[source],
+            h_s.at[source],
+            h_r.at[source],
+            source,
+            core,
+        ).wait()
+    loads[3].wait()
+    hidden = jnp.transpose(hidden_in[...].reshape(n * cols, rows))
+    chunk = 512
+
+    def descend(step, carry):
+        at = pl.ds(pl.multiple_of(step * chunk, chunk), chunk)
+        sums_out[:, at] = jnp.dot(
+            hidden, down_ref[:, at], preferred_element_type=jnp.float32
+        ).astype(BF)
+        return carry
+
+    lax.fori_loop(0, width // chunk, descend, 0)
+    swap = send(sums_out, sums_in, pair_s.at[3], pair_r.at[3], me, 1 - core)
+    swap.start()
+    swap.wait()
+    pre = ALPHA * first_ref[...].reshape(rows, width).astype(jnp.float32) + (
+        sums_out[...].astype(jnp.float32) + sums_in[...].astype(jnp.float32)
+    )
+    center = jnp.mean(pre, axis=1, keepdims=True)
+    shifted = pre - center
+    spread = jnp.mean(shifted * shifted, axis=1, keepdims=True)
+    pre_ref[...] = shifted * lax.rsqrt(spread + EPS_NORM)
+    half = pre_ref[:, pl.ds(pl.multiple_of(core * columns, columns), columns)]
+    out_ref[...] = (half * gain2_ref[...]).astype(BF)
+
+
+def layer(n, small, large, resid, latents, width, sizes):
+    rows, columns = resid.shape
+    lat_width, cols, down = sizes
+    dma = pltpu.SemaphoreType.DMA
+    vmem = pl.BlockSpec(memory_space=pltpu.VMEM)
+    anywhere = pl.BlockSpec(memory_space=pl.ANY)
+    heads = large[0].shape[0]
+    gather_sems = [dma((n // 4,))] * 10 + [dma((n,))] * 2
+    return pl.pallas_call(
+        functools.partial(layer_kernel, n),
+        out_shape=jax.ShapeDtypeStruct((rows, columns), BF),
+        in_specs=[vmem] * len(small) + [anywhere] * len(large),
+        out_specs=vmem,
+        scratch_shapes=[
+            pltpu.VMEM((n,) + latents, BF),
+            pltpu.VMEM((n, rows, lat_width + LANES), BF),
+            pltpu.VMEM((rows, large[0].shape[0]), jnp.float32),
+            pltpu.VMEM((rows, large[1].shape[0]), jnp.float32),
+            pltpu.VMEM(large[0].shape, BF),
+            pltpu.VMEM(large[1].shape, BF),
+            pltpu.VMEM((2, cols, width), BF),
+            pltpu.VMEM((rows, width), BF),
+            pltpu.VMEM((rows, width), BF),
+            pltpu.VMEM((rows, LANES), jnp.float32),
+            pltpu.VMEM((rows, LANES), jnp.float32),
+            pltpu.VMEM(resid.shape, BF),
+            pltpu.VMEM((2, rows // 2, width), BF),
+            pltpu.VMEM((n, 2, rows // 2, width), BF),
+            pltpu.VMEM((n, 2 * cols, rows), BF),
+            pltpu.VMEM((n, cols, rows), BF),
+            pltpu.VMEM((n, cols, rows), BF),
+            pltpu.VMEM(down, BF),
+            pltpu.VMEM((rows, width), BF),
+            pltpu.VMEM((rows, width), BF),
+            pltpu.VMEM((rows, width), jnp.float32),
+            dma((4,)),
+            dma((4,)),
+            dma((4,)),
+        ]
+        + [dma((n,))] * 4
+        + gather_sems * 2,
+        compiler_params=pltpu.CompilerParams(
+            collective_id=0, has_side_effects=True, vmem_limit_bytes=60 * 1024 * 1024
+        ),
+    )(*small, *large)
+
+
+def pack(lat_n, k_rot):
+    parts = [lat_n[:, at : at + LANES] for at in range(0, lat_n.shape[1], LANES)]
+    groups = LANES // DR
+    k_packed = k_rot.reshape(groups, -1, DR).transpose(1, 0, 2).reshape(-1, LANES)
+    whole = jnp.concatenate(parts + [k_packed], axis=0)
+    return whole.reshape(2, whole.shape[0] // 2, LANES)
+
+
+def direct_fits(resid, latent, ffn_gate, n):
+    return (
+        lax.axis_size("tp") == 2
+        and n % 4 == 0
+        and resid.shape[0] == LANES
+        and resid.shape[1] % LANES == 0
+        and latent.shape[1] % LANES == 0
+        and ffn_gate.shape[0] == LANES
+        and ffn_gate.shape[1] % (16 * n) == 0
+    )
 
 
 def shards(
@@ -101,6 +609,40 @@
     heads_b = qb_nope.shape[1] // DB
     lat_n = rms_scale(latent, lat_gain).astype(jnp.bfloat16)
     k_rot = rotary(key_rope.astype(jnp.float32), positions).astype(jnp.bfloat16)
+    n = lax.axis_size("sp")
+    if direct_fits(resid, latent, ffn_gate, n):
+        cols = ffn_gate.shape[1] // n
+        start = lax.axis_index("sp") * cols
+        taps = jnp.concatenate(
+            [lax.dynamic_slice_in_dim(taps, start, cols, 1).T for taps in (conv_gate, conv_val)]
+        )
+        spot = jnp.arange(LANES) % DR
+        freq = THETA ** (-(spot % (DR // 2)).astype(jnp.float32) * 2.0 / DR)
+        angle = positions.astype(jnp.float32)[:, None] * freq[None, :]
+        turn = jnp.where(spot < DR // 2, -1.0, 1.0)[None, :]
+        packed = pack(lat_n, k_rot)
+        small = (
+            packed,
+            qa_nope,
+            qb_nope,
+            qa_rope,
+            qb_rope,
+            jnp.cos(angle),
+            jnp.sin(angle) * turn,
+            wa_key,
+            wa_val,
+            wb_key,
+            wb_val,
+            gain_a[None],
+            gain_b[None],
+            resid,
+            norm1_gain[None],
+            taps,
+            norm2_gain[None],
+        )
+        large = (wa_out, wb_out, ffn_down, jnp.stack([ffn_gate.T, ffn_val.T]))
+        sizes = (latent.shape[1], cols, ffn_down.shape)
+        return layer(n, small, large, resid, packed.shape, wa_out.shape[1], sizes)
     rot_a = rotary(qa_rope.astype(jnp.float32).reshape(tok_rows, heads_a, DR), positions).astype(
         jnp.bfloat16
     )

time: 422 us -> 134 us (0.32)
  waiting for transfers between devices: 314 us -> 0 us
  Pallas kernels: 0 us -> 124 us
  blocking collectives: 41.3 us -> 0 us
  matrix products: 33.3 us -> 0 us
  between operations: 13.5 us -> 0.08 us
  other arithmetic: 10.8 us -> 5.79 us
    all_gather x3 -> x0, waiting for transfers between devices: 290 us -> none  [the longest x1 135 us: shards(): lax.all_gather(ffn_val, 'sp', axis=0, tiled=True)]
    pallas_call x0 -> x1, Pallas kernels: none -> 124 us  [layer(): pl.pallas_call(functools.partial(layer_kernel, n), out_shape=jax.ShapeDty...]
    dot_general x15 -> x0, matrix products: 33.3 us -> none  [the longest x1 7.93 us: shards(): down = jnp.dot(hidden, ffn_down, preferred_element_type=jnp.float32)]
    all_gather x2 -> x0, blocking collectives: 31.3 us -> none  [the longest x1 29.1 us: shards(): lax.all_gather(k_rot, 'sp', axis=0, tiled=True)]
    reduce_scatter x2 -> x0, waiting for transfers between devices: 19.8 us -> none  [the longest x1 11.8 us: shards(): lax.psum_scatter(down.astype(jnp.bfloat16), 'tp', scatter_dimension=1, ti...]
    psum x3 -> x0, blocking collectives: 10 us -> none  [the longest x1 5.1 us: shards(): energy = lax.psum(local_energy, 'tp')]
  transfers between devices with their start and end apart: 7 -> 0, of which waited for: 6 -> 0; matrix products, arithmetic and copies ran while one was open for 4% -> 0% of each run, Pallas kernels for 0% -> 0%
where the time goes in v1:
time: 134 us
  Pallas kernels  124 us (93%)
  other arithmetic  5.79 us (4%)
  local copies, waits for them, and re-layouts  4.35 us (3%)
    pallas_call x1, Pallas kernels, layer(): pl.pallas_call(functools.partial(layer_kernel, n), out_shape=jax.ShapeDty...  124 us

profile of v1, /device:TPU:31, one launch (start us, length us, event | category | flops | bytes accessed | tf_op | source)
XLA Modules:
  0.0 133.8 jit_solution(6055037843103666116)
XLA Ops:
  0.0 0.0 copy-start
  0.0 0.0 copy-start.1
  0.0 1.1 fusion
  1.1 0.8 dynamic-slice_bitcast_fusion
  1.9 0.1 pad_maximum_fusion.2
  2.0 0.7 convert_element_type.28
  2.7 0.1 fusion.9
  2.8 0.1 concatenate.15
  2.9 0.1 concatenate.16
  3.0 0.1 copy.29
  3.1 0.1 reshape.59
  3.2 0.9 fusion.2
  4.2 0.6 pad_maximum_fusion.1
  4.8 1.0 fusion.3
  5.7 0.8 copy.32.taps_ref
  6.6 0.0 copy-done
  6.6 0.3 copy.30
  6.9 0.0 copy-done.1
  6.9 0.3 copy.31
  7.3 1.3 pad_maximum_fusion.columns_hbm
  8.5 123.5 %shard_map.217 = bf16[128,1024]{1,0:T(8,128)(2,1)} custom-call(bf16[2,144,128]{2,1,0:T(8,128)(2,1)} %bitcast.23, bf16[128,512]{1,0:T(8,128)(2,1)} %qa_ref.1, bf16[128,512]{1,0:T(8,128)(2,1)} %qb_ref.1, bf16[128,256]{1,0:T(8,128)(2,1)} %ra_ref.1, bf16[128,128]{1,0:T(8,128)(2,1)} %rb_ref.1, f32[128,128]{1,0:T(8,128)} %get-tuple-element.10.cos_ref, ...), custom_call_target="tpu_custom_call" | custom-call | tf_op jit(solution)/shard_map/pallas_call | solution.py:522
  132.1 1.7 %copy.34 = bf16[128,1024]{1,0:T(8,128)(2,1)} copy(bf16[128,1024]{1,0:T(8,128)(2,1)} %shard_map.217) | data formatting | bytes 524288
  (6 shorter events, 0.1 us)
Async XLA Ops:
  0.0 6.6 %copy-start = (bf16[128,2816]{1,0:T(8,128)(2,1)S(1)}, bf16[128,2816]{1,0:T(8,128)(2,1)}, u32[]{:S(2)}) copy-start(bf16[128,2816]{1,0:T(8,128)(2,1)} %param.40) | copy-start | bytes 2162692
  0.0 6.9 %copy-start.1 = (bf16[128,2816]{1,0:T(8,128)(2,1)S(1)}, bf16[128,2816]{1,0:T(8,128)(2,1)}, u32[]{:S(2)}) copy-start(bf16[128,2816]{1,0:T(8,128)(2,1)} %param.41) | copy-start | bytes 2162692
